TPU v7x, 512 devices: a whole 4x8x8 slice. The times are simulated.
512 devices in a mesh: ep: 32 (over z, x), tp: 16 (over y, core).
Axes of the slice: x: 4, y: 8, z: 8, core: 2. Of those that a mesh axis runs over, the one named last changes fastest.
Arguments:
- query_rows: bfloat16 [16384, 3072], P('ep', 'tp'), may hold values from -6 to 6
- key_rows: bfloat16 [16384, 1024], P('ep', 'tp'), may hold values from -6 to 6
- value_rows: bfloat16 [16384, 1024], P('ep', 'tp'), may hold values from -6 to 6
- query_gain: float32 [48, 64], P('tp'), may hold values from 0.4 to 48
- key_gain: float32 [16, 64], P('tp'), may hold values from 0.1 to 1.9
- sink_logits: float32 [48], P('tp'), may hold values from 1 to 6
- out_weight: bfloat16 [3072, 2048], P('tp'), may hold values from -0.109375 to 0.109375
- expert_input: bfloat16 [16384, 2048], P(('ep', 'tp')), may hold values from -6 to 6
- expert_gain: float32 [2048], replicated, may hold values from 0.1 to 1.9
- routes: int32 [16384, 2], P(('ep', 'tp')), may hold values from 0 to 31, all different within a row; in each aligned block of 32 rows (0 to 31, 32 to 63, ...) at most 3 rows name the same one
- route_logits: float32 [16384, 2], P(('ep', 'tp')), may hold values from -6 to 6
- gate_weight: bfloat16 [32, 2048, 2048], P('ep', None, 'tp'), may hold values from -0.375 to 0.375
- up_weight: bfloat16 [32, 2048, 2048], P('ep', None, 'tp'), may hold values from -0.375 to 0.375
- down_weight: bfloat16 [32, 2048, 2048], P('ep', 'tp'), may hold values from -0.01953125 to 0.01953125
Outputs:
- attended: bfloat16 [16384, 2048], P(('ep', 'tp'))
- expert_mix: bfloat16 [16384, 2048], P(('ep', 'tp'))
Inputs may be any that keep to these rules, and one draw needn't show every extreme that they name: `routes`: each row names 2 different experts; in the rows of one device no expert is named more than 3 times, and in some device one expert is named exactly 3 times.
All inputs are finite; a program needn't handle non-finite values.
Results may differ from a plain program's by a relative error of at most 0.017.
The roundings to bfloat16 on the way count: a program that leaves them out, or rounds other values in their place, can miss the bound.
Values may be sent and summed in bfloat16 or wider, within the bound.
A program may use at most 64 MiB of HBM per device.

v0:
```python
import jax
import jax.numpy as jnp
from jax import lax
from jax.sharding import PartitionSpec as P

EXPERTS = 32
WINDOW = 128
EPSILON = 1e-06
CLAMP_LIMIT = 7.0
ACT_SLOPE = 1.702
NEGATIVE = -1e30


def shifted(value, axis, steps):
    count = lax.axis_size(axis)
    initial, last = (max(0, -steps), min(count, count - steps))
    return lax.ppermute(value, axis, [(source, source + steps) for source in range(initial, last)])


def head_norm(row_data, gain_table):
    head_count, head_size = gain_table.shape
    widened = row_data.astype(jnp.float32).reshape(row_data.shape[0], head_count, head_size)
    scaled = widened * lax.rsqrt(jnp.mean(widened * widened, axis=-1, keepdims=True) + EPSILON)
    return (scaled * gain_table).astype(jnp.bfloat16)


def band(padded, blocks):
    tiled = padded.reshape((blocks + 1, WINDOW) + padded.shape[1:])
    return jnp.concatenate([tiled[:-1], tiled[1:]], axis=1)


def attend(query_rows, key_rows, value_rows, query_gain, key_gain, sink_logits):
    seq_rows = query_rows.shape[0]
    key_heads, head_size = key_gain.shape
    group_size = query_gain.shape[0] // key_heads
    blocks = seq_rows // WINDOW
    query_hat = head_norm(query_rows, query_gain).reshape(
        blocks, WINDOW, key_heads, group_size, head_size
    )
    key_hat = head_norm(key_rows, key_gain)
    value_hat = value_rows.reshape(seq_rows, key_heads, head_size)
    tail_rows = jnp.stack([key_hat[seq_rows - WINDOW :], value_hat[seq_rows - WINDOW :]])
    earlier = shifted(tail_rows, "ep", 1)
    key_band = band(jnp.concatenate([earlier[0], key_hat], axis=0), blocks)
    value_band = band(jnp.concatenate([earlier[1], value_hat], axis=0), blocks)
    query_pos = lax.broadcasted_iota(jnp.int32, (WINDOW, 2 * WINDOW), 0)
    key_pos = lax.broadcasted_iota(jnp.int32, (WINDOW, 2 * WINDOW), 1)
    distance = query_pos + WINDOW - key_pos
    inside = (distance >= 0) & (distance < WINDOW)
    first_block = (lax.broadcasted_iota(jnp.int32, (blocks, 1, 1), 0) == 0) & (
        lax.axis_index("ep") == 0
    )
    allowed = inside[None] & ~(first_block & (key_pos < WINDOW)[None])
    scores = jnp.einsum(
        "bqkgd,bjkd->bkgqj", query_hat, key_band, preferred_element_type=jnp.float32
    ) * head_size ** (-0.5)
    scores = jnp.where(allowed[:, None, None], scores, NEGATIVE)
    sink_table = sink_logits.reshape(1, key_heads, group_size, 1, 1)
    highest = jnp.maximum(jnp.max(scores, axis=-1, keepdims=True), sink_table)
    weights = jnp.exp(scores - highest)
    total = jnp.sum(weights, axis=-1, keepdims=True) + jnp.exp(sink_table - highest)
    mixed = jnp.einsum(
        "bkgqj,bjkd->bkgqd",
        weights.astype(jnp.bfloat16),
        value_band,
        preferred_element_type=jnp.float32,
    )
    mixed = (mixed / total).astype(jnp.bfloat16)
    return jnp.transpose(mixed, (0, 3, 1, 2, 4)).reshape(seq_rows, -1)


def slot_maps(route_block, capacity):
    flat_routes = route_block.reshape(-1)
    expert_hot = (flat_routes[:, None] == lax.broadcasted_iota(jnp.int32, (1, EXPERTS), 1)).astype(
        jnp.int32
    )
    before = jnp.cumsum(expert_hot, axis=0) - expert_hot
    position = jnp.sum(before * expert_hot, axis=1)
    place_hot = (position[:, None] == lax.broadcasted_iota(jnp.int32, (1, capacity), 1)).astype(
        jnp.float32
    )
    row_total, fanout = route_block.shape
    return (
        expert_hot.astype(jnp.float32).reshape(row_total, fanout, EXPERTS),
        place_hot.reshape(row_total, fanout, capacity),
    )


def dispatch_matrix(route_block, capacity):
    expert_hot, place_hot = slot_maps(route_block, capacity)
    return jnp.einsum("rke,rkc->ecr", expert_hot, place_hot).astype(jnp.bfloat16)


def combine_matrix(route_block, route_weight, capacity):
    expert_hot, place_hot = slot_maps(route_block, capacity)
    return jnp.einsum("rke,rkc,rk->rec", expert_hot, place_hot, route_weight)


def expert_hidden(piece, gate_weight, up_weight):
    gate_pre = jnp.einsum("aecd,edf->aecf", piece, gate_weight, preferred_element_type=jnp.float32)
    up_pre = jnp.einsum("aecd,edf->aecf", piece, up_weight, preferred_element_type=jnp.float32)
    clipped = jnp.minimum(gate_pre, CLAMP_LIMIT)
    linear = jnp.clip(up_pre, -CLAMP_LIMIT, CLAMP_LIMIT)
    return (clipped * jax.nn.sigmoid(ACT_SLOPE * clipped) * (linear + 1.0)).astype(jnp.bfloat16)


def on_device(
    query_rows,
    key_rows,
    value_rows,
    query_gain,
    key_gain,
    sink_logits,
    out_weight,
    expert_input,
    expert_gain,
    routes,
    route_logits,
    gate_weight,
    up_weight,
    down_weight,
):
    heads_out = attend(query_rows, key_rows, value_rows, query_gain, key_gain, sink_logits)
    attended = lax.psum_scatter(
        jnp.dot(heads_out, out_weight, preferred_element_type=jnp.float32).astype(jnp.bfloat16),
        "tp",
        scatter_dimension=0,
        tiled=True,
    )
    own_rows = expert_input.shape[0]
    fanout = routes.shape[1]
    capacity = (3 * own_rows * fanout + 2 * EXPERTS - 1) // (2 * EXPERTS)
    ep_size = lax.axis_size("ep")
    tp_size = lax.axis_size("tp")
    local_experts = gate_weight.shape[0]
    widened = expert_input.astype(jnp.float32)
    normed = (
        widened
        * lax.rsqrt(jnp.mean(widened * widened, axis=-1, keepdims=True) + EPSILON)
        * expert_gain
    ).astype(jnp.bfloat16)
    route_weight = jax.nn.softmax(route_logits, axis=-1)
    combine = combine_matrix(routes, route_weight, capacity)
    sender = dispatch_matrix(routes, capacity)
    slot_rows = jnp.einsum(
        "ecr,rd->ecd", sender, normed, preferred_element_type=jnp.float32
    ).astype(jnp.bfloat16)
    slot_rows = slot_rows.reshape(ep_size, local_experts, capacity, -1)
    arrived = lax.all_to_all(slot_rows, "ep", split_axis=0, concat_axis=0, tiled=True)
    hidden_units = expert_hidden(
        lax.all_gather(arrived, "tp", axis=0, tiled=True), gate_weight, up_weight
    )
    partial_value = jnp.einsum(
        "aecf,efd->aecd", hidden_units, down_weight, preferred_element_type=jnp.float32
    ).astype(jnp.bfloat16)
    partial_value = partial_value.reshape(tp_size, ep_size * local_experts * capacity, -1)
    pieces = lax.all_to_all(partial_value, "tp", split_axis=0, concat_axis=0, tiled=True)
    summed = jnp.sum(pieces, axis=0, dtype=jnp.float32).astype(jnp.bfloat16)
    summed = summed.reshape(ep_size, local_experts * capacity, -1)
    returned = lax.all_to_all(summed, "ep", split_axis=0, concat_axis=0, tiled=True)
    expert_mix = jnp.einsum("rec,ecd->rd", combine, returned.astype(jnp.float32)).astype(
        jnp.bfloat16
    )
    return (attended, expert_mix)


def solution(mesh):
    placed = (
        P("ep", "tp"),
        P("ep", "tp"),
        P("ep", "tp"),
        P("tp", None),
        P("tp", None),
        P("tp"),
        P("tp", None),
        P(("ep", "tp"), None),
        P(),
        P(("ep", "tp"), None),
        P(("ep", "tp"), None),
        P("ep", None, "tp"),
        P("ep", None, "tp"),
        P("ep", "tp", None),
    )
    return jax.shard_map(
        on_device,
        mesh=mesh,
        in_specs=placed,
        out_specs=(P(("ep", "tp"), None), P(("ep", "tp"), None)),
        check_vma=False,
    )
```

profile of v0, /device:TPU:24, one launch (start us, length us, event | category | flops | bytes accessed | tf_op | source)
XLA Modules:
  0.0 328.0 jit_solution(9556012948772609825)
XLA Ops:
  7.2 1.1 fusion.58
  8.3 0.8 copy.42
  9.7 0.4 fusion.34
  10.1 1.2 fusion.4
  11.6 30.7 %all_to_all.15 = bf16[32,1,3,2048]{3,2,1,0:T(4,128)(2,1)S(1)} all-to-all(bf16[32,1,3,2048]{3,2,1,0:T(4,128)(2,1)S(1)} %copy.46), channel_id=1, replica_groups=mesh['ep'=32,'tp'=16] {'ep'}, dimensions={0} | all-to-all | bytes 786432 | tf_op jit(solution)/shard_map/all_to_all | solution.py:149
  42.3 1.1 copy.47
  43.5 44.1 %all-gather.2.cloned.1.call-done = bf16[512,1,3,2048]{3,0,2,1:T(8,128)(2,1)} async-done(((bf16[32,1,3,2048]{3,0,2,1:T(8,128)(2,1)}), bf16[512,1,3,2048]{3,0,2,1:T(8,128)(2,1)}) %all-gather.2.cloned.1.call-update) | async-done | bytes 6291472 | tf_op jit(solution)/shard_map/all_gather | solution.py:151
  87.5 4.6 %fusion.11 = f32[512,1,3,128]{3,0,2,1:T(8,128)S(1)} fusion(bf16[512,1,3,2048]{3,0,2,1:T(8,128)(2,1)} %all-gather.2.cloned.1.call-done, bf16[1,2048,128]{2,1,0:T(8,128)(2,1)S(1)} %copy-done.9), kind=kOutput, calls=%fused_computation.15 | convolution fusion | flops 805502976 | bytes 7602176 | tf_op jit(solution)/shard_map/aecd,edf->aecf/dot_general | solution.py:100
  92.1 11.9 %convert_bitcast_fusion = bf16[512,1,3,2048]{3,0,2,1:T(8,128)(2,1)} fusion(bf16[512,1,3,2048]{3,0,2,1:T(8,128)(2,1)} %all-gather.2.cloned.1.call-done, f32[512,1,3,128]{3,0,2,1:T(8,128)S(1)} %fusion.11, bf16[1,128,2048]{2,1,0:T(8,128)(2,1)S(1)} %copy-done.3, bf16[1,2048,128]{2,1,0:T(8,128)(2,1)S(1)} %copy-done.4), kind=kOutput, calls=%fused_computation.4 | convolution fusion | flops 1615527936 | bytes 14417920 | tf_op jit(solution)/shard_map/aecf,efd->aecd/dot_general | solution.py:153
  104.1 11.6 %copy.48 = bf16[512,1,3,2048]{3,2,0,1:T(4,128)(2,1)} copy(bf16[512,1,3,2048]{3,0,2,1:T(8,128)(2,1)} %convert_bitcast_fusion) | data formatting | bytes 12582912 | tf_op jit(solution)/shard_map/convert_element_type | solution.py:155
  115.6 16.3 %reshape.224 = bf16[16,96,2048]{2,1,0:T(8,128)(2,1)} reshape(bf16[512,1,3,2048]{3,2,0,1:T(4,128)(2,1)} %copy.48) | data formatting | bytes 12582912 | tf_op jit(solution)/shard_map/reshape | solution.py:156
  132.0 5.5 %all-to-all-start.1 = ((bf16[16,96,2048]{2,1,0:T(8,128)(2,1)}), bf16[16,96,2048]{2,1,0:T(8,128)(2,1)}, u32[]{:S(2)}, u32[]{:S(2)}) async-start(bf16[16,96,2048]{2,1,0:T(8,128)(2,1)} %reshape.224), calls=%async_computation.2 | async-start | bytes 12582912 | tf_op jit(solution)/shard_map/all_to_all | solution.py:157
  137.7 3.4 %collective-permute-start = (bf16[2,128,1,64]{1,3,2,0:T(8,128)(2,1)S(1)}, bf16[2,128,1,64]{1,3,2,0:T(8,128)(2,1)S(1)}, u32[]{:S(2)}, u32[]{:S(2)}) collective-permute-start(bf16[2,128,1,64]{1,3,2,0:T(8,128)(2,1)S(1)} %pad_maximum_fusion.2), channel_id=1, source_target_pairs={{0,16},{16,32},{32,48},{48,64},{64,80},{80,96},{96,112},{112,128},... | collective-permute-start | bytes 98312 | tf_op jit(solution)/shard_map/ppermute | solution.py:17
  141.8 0.9 collective-permute-done
  142.7 0.5 fusion.105
  143.6 0.4 fusion.33
  144.1 2.1 convolution_convert_fusion
  146.3 140.4 %all-to-all-done.1 = bf16[16,96,2048]{2,1,0:T(8,128)(2,1)} async-done(((bf16[16,96,2048]{2,1,0:T(8,128)(2,1)}), bf16[16,96,2048]{2,1,0:T(8,128)(2,1)}, u32[]{:S(2)}, u32[]{:S(2)}) %all-to-all-start.1) | async-done | bytes 6291488 | tf_op jit(solution)/shard_map/all_to_all | solution.py:157
  286.7 4.1 %reduce_sum.76 = bf16[96,2048]{1,0:T(8,128)(2,1)S(1)} reduce(bf16[16,96,2048]{2,1,0:T(8,128)(2,1)} %all-to-all-done.1, bf16[]{:T(256)} %constant.49.clone.1), dimensions={0}, to_apply=%region_10.11 | reduce | flops 2949120 | bytes 6684674 | tf_op jit(solution)/shard_map/reduce_sum | solution.py:158
  290.8 1.0 reshape.225
  291.8 10.2 %all-to-all-start.2 = ((bf16[32,3,2048]{2,1,0:T(4,128)(2,1)}), bf16[32,3,2048]{2,1,0:T(4,128)(2,1)S(1)}, u32[]{:S(2)}, u32[]{:S(2)}) async-start(bf16[32,3,2048]{2,1,0:T(4,128)(2,1)} %reshape.225), calls=%async_computation.3 | async-start | bytes 1048576 | tf_op jit(solution)/shard_map/all_to_all | solution.py:160
  302.2 0.4 fusion.84
  302.5 17.5 %all-to-all-done.2 = bf16[32,3,2048]{2,1,0:T(4,128)(2,1)S(1)} async-done(((bf16[32,3,2048]{2,1,0:T(4,128)(2,1)}), bf16[32,3,2048]{2,1,0:T(4,128)(2,1)S(1)}, u32[]{:S(2)}, u32[]{:S(2)}) %all-to-all-start.2) | async-done | bytes 393248 | tf_op jit(solution)/shard_map/all_to_all | solution.py:160
  320.1 1.1 fusion.5
  (64 shorter events, 2.5 us)
Async XLA Ops:
  7.2 137.0 %copy-start = (bf16[192,2048]{1,0:T(8,128)(2,1)S(1)}, bf16[192,2048]{1,0:T(8,128)(2,1)}, u32[]{:S(2)}) copy-start(bf16[192,2048]{1,0:T(8,128)(2,1)} %param.20) | copy-start | bytes 2359300
  7.2 80.4 %all-gather.2.cloned.1.call-start = ((), (), s32[]{:S(2)}) async-start(), calls=%async_computation.5 | async-start | bytes 6684672 | tf_op jit(solution)/shard_map/all_gather | solution.py:151
  9.7 77.9 %copy-start.9 = (bf16[1,2048,128]{2,1,0:T(8,128)(2,1)S(1)}, bf16[1,2048,128]{2,1,0:T(8,128)(2,1)}, u32[]{:S(2)}) copy-start(bf16[1,2048,128]{2,1,0:T(8,128)(2,1)} %param.25) | copy-start | bytes 1572868
  43.4 48.7 %copy-start.3 = (bf16[1,128,2048]{2,1,0:T(8,128)(2,1)S(1)}, bf16[1,128,2048]{2,1,0:T(8,128)(2,1)}, u32[]{:S(2)}) copy-start(bf16[1,128,2048]{2,1,0:T(8,128)(2,1)} %param.27) | copy-start | bytes 1572868
  43.4 48.7 %copy-start.4 = (bf16[1,2048,128]{2,1,0:T(8,128)(2,1)S(1)}, bf16[1,2048,128]{2,1,0:T(8,128)(2,1)}, u32[]{:S(2)}) copy-start(bf16[1,2048,128]{2,1,0:T(8,128)(2,1)} %param.26) | copy-start | bytes 1572868
  131.9 5.6 %copy-start.2 = (bf16[512,64]{0,1:T(8,128)(2,1)S(1)}, bf16[512,64]{0,1:T(8,128)(2,1)}, u32[]{:S(2)}) copy-start(bf16[512,64]{0,1:T(8,128)(2,1)} %param.15) | copy-start | bytes 196612
  132.0 5.6 %copy-start.7 = (f32[1,64]{1,0:T(1,128)S(1)}, f32[1,64]{1,0:T(1,128)}, u32[]{:S(2)}) copy-start(f32[1,64]{1,0:T(1,128)} %param.18) | copy-start | bytes 772
  132.0 5.7 %copy-start.5 = (bf16[512,64]{0,1:T(8,128)(2,1)S(1)}, bf16[512,64]{0,1:T(8,128)(2,1)}, u32[]{:S(2)}) copy-start(bf16[512,64]{0,1:T(8,128)(2,1)} %param.16) | copy-start | bytes 196612
  132.0 9.1 %copy-start.1 = (bf16[512,192]{0,1:T(8,128)(2,1)S(1)}, bf16[512,192]{0,1:T(8,128)(2,1)}, u32[]{:S(2)}) copy-start(bf16[512,192]{0,1:T(8,128)(2,1)} %param.14) | copy-start | bytes 589828
  132.0 154.7 %all-to-all-start.1 = ((bf16[16,96,2048]{2,1,0:T(8,128)(2,1)}), bf16[16,96,2048]{2,1,0:T(8,128)(2,1)}, u32[]{:S(2)}, u32[]{:S(2)}) async-start(bf16[16,96,2048]{2,1,0:T(8,128)(2,1)} %reshape.224), calls=%async_computation.2 | async-start | bytes 12582912 | tf_op jit(solution)/shard_map/all_to_all | solution.py:157
  137.5 5.3 %copy-start.10 = (f32[3,64]{1,0:T(4,128)S(1)}, f32[3,64]{1,0:T(4,128)}, u32[]{:S(2)}) copy-start(f32[3,64]{1,0:T(4,128)} %param.17) | copy-start | bytes 2308
  137.5 183.7 %reduce-scatter.2.cloned.1.call-start = ((), (), s32[]{:S(2)}) async-start(), calls=%async_computation.4 | async-start | bytes 2228224 | tf_op jit(solution)/shard_map/reduce_scatter | solution.py:124
  137.7 5.0 %collective-permute-start = (bf16[2,128,1,64]{1,3,2,0:T(8,128)(2,1)S(1)}, bf16[2,128,1,64]{1,3,2,0:T(8,128)(2,1)S(1)}, u32[]{:S(2)}, u32[]{:S(2)}) collective-permute-start(bf16[2,128,1,64]{1,3,2,0:T(8,128)(2,1)S(1)} %pad_maximum_fusion.2), channel_id=1, source_target_pairs={{0,16},{16,32},{32,48},{48,64},{64,80},{80,96},{96,112},{112,128},... | collective-permute-start | bytes 98312 | tf_op jit(solution)/shard_map/ppermute | solution.py:17
  141.2 2.0 copy-start.8
  146.3 155.7 %copy-start.6 = (f32[32,2]{0,1:T(2,128)S(1)}, f32[32,2]{0,1:T(2,128)}, u32[]{:S(2)}) copy-start(f32[32,2]{0,1:T(2,128)} %param.24) | copy-start | bytes 772
  291.8 28.3 %all-to-all-start.2 = ((bf16[32,3,2048]{2,1,0:T(4,128)(2,1)}), bf16[32,3,2048]{2,1,0:T(4,128)(2,1)S(1)}, u32[]{:S(2)}, u32[]{:S(2)}) async-start(bf16[32,3,2048]{2,1,0:T(4,128)(2,1)} %reshape.225), calls=%async_computation.3 | async-start | bytes 1048576 | tf_op jit(solution)/shard_map/all_to_all | solution.py:160
Sparse Core Ops, SparseCore 0:
  43.6 43.9 all-gather.1
  146.4 136.6 reduce-scatter.1
where the time goes:
time: 329 us; the launch traced here: 328 us
  waiting for transfers between devices  203 us (62%)
  local copies, waits for them, and re-layouts  31.8 us (10%)
  blocking collectives  30.7 us (9%)
  matrix products  22.5 us (7%)
  starting transfers between devices  19.1 us (6%)
  between operations  14.4 us (4%)
  other arithmetic  6.53 us (2%)
    all_to_all x1, waiting for transfers between devices, on_device(): lax.all_to_all(partial_value, 'tp', split_axis=0, concat_axis=0, tiled=True)  140 us
    all_gather x1, waiting for transfers between devices, on_device(): lax.all_gather(arrived, 'tp', axis=0, tiled=True)  44.1 us
    all_to_all x1, blocking collectives, on_device(): lax.all_to_all(slot_rows, 'ep', split_axis=0, concat_axis=0, tiled=True)  30.7 us
    all_to_all x1, waiting for transfers between devices, on_device(): lax.all_to_all(summed, 'ep', split_axis=0, concat_axis=0, tiled=True)  17.5 us
    reshape x1, local copies, waits for them, and re-layouts, on_device(): partial_value.reshape(tp_size, ep_size * local_experts * capacity, -1)  16.3 us
    dot_general x1, matrix products, on_device(): jnp.einsum('aecf,efd->aecd', hidden_units, down_weight, preferred_element...  11.9 us
    convert_element_type x1, local copies, waits for them, and re-layouts, on_device(): partial_value = jnp.einsum('aecf,efd->aecd', hidden_units, down_weight, p...  11.6 us
    all_to_all x1, starting transfers between devices, on_device(): lax.all_to_all(summed, 'ep', split_axis=0, concat_axis=0, tiled=True)  10.2 us
  transfers between devices with their start and end apart: 5, of which 4 were waited for; matrix products, arithmetic and copies ran while one was open for 3% of the time, Pallas kernels for 0%

commit v1 on v0

--- a/solution.py
+++ b/solution.py
@@ -9,6 +9,11 @@
 CLAMP_LIMIT = 7.0
 ACT_SLOPE = 1.702
 NEGATIVE = -1e30
+
+
+def gather_by_exchange(array, axis, dim):
+    copies = jnp.concatenate([array] * lax.axis_size(axis), axis=dim)
+    return lax.all_to_all(copies, axis, dim, dim, tiled=True)
 
 
 def shifted(value, axis, steps):
@@ -147,9 +152,7 @@
     ).astype(jnp.bfloat16)
     slot_rows = slot_rows.reshape(ep_size, local_experts, capacity, -1)
     arrived = lax.all_to_all(slot_rows, "ep", split_axis=0, concat_axis=0, tiled=True)
-    hidden_units = expert_hidden(
-        lax.all_gather(arrived, "tp", axis=0, tiled=True), gate_weight, up_weight
-    )
+    hidden_units = expert_hidden(gather_by_exchange(arrived, "tp", 0), gate_weight, up_weight)
     partial_value = jnp.einsum(
         "aecf,efd->aecd", hidden_units, down_weight, preferred_element_type=jnp.float32
     ).astype(jnp.bfloat16)

time: 329 us -> 484 us (1.47)
  blocking collectives: 30.7 us -> 221 us
  waiting for transfers between devices: 203 us -> 159 us
  matrix products: 22.5 us -> 29.5 us
  local copies, waits for them, and re-layouts: 31.8 us -> 38.2 us
  starting transfers between devices: 19.1 us -> 13.3 us
    all_to_all x0 -> x1, blocking collectives: none -> 191 us  [gather_by_exchange(): return lax.all_to_all(copies, axis, dim, dim, tiled=True)]
    all_gather x1 -> x0, waiting for transfers between devices: 44.1 us -> none  [on_device(): lax.all_gather(arrived, 'tp', axis=0, tiled=True)]
    unnamed x23 -> x40, local copies, waits for them, and re-layouts: 0.83 us -> 8.16 us
    all_to_all x1, starting transfers between devices: 10.2 us -> 4.64 us  [on_device(): lax.all_to_all(summed, 'ep', split_axis=0, concat_axis=0, tiled=True)]
  transfers between devices with their start and end apart: 5 -> 4, of which waited for: 4 -> 3; matrix products, arithmetic and copies ran while one was open for 3% -> 2% of each run, Pallas kernels for 0% -> 0%
where the time goes in v1:
time: 484 us; the launch traced here: 483 us
  blocking collectives  221 us (46%)
  waiting for transfers between devices  159 us (33%)
  local copies, waits for them, and re-layouts  38.2 us (8%)
  matrix products  29.5 us (6%)
  between operations  14.5 us (3%)
  starting transfers between devices  13.3 us (3%)
  other arithmetic  6.47 us (1%)
    all_to_all x1, blocking collectives, gather_by_exchange(): return lax.all_to_all(copies, axis, dim, dim, tiled=True)  191 us
    all_to_all x1, waiting for transfers between devices, on_device(): lax.all_to_all(partial_value, 'tp', split_axis=0, concat_axis=0, tiled=True)  141 us
    all_to_all x1, blocking collectives, on_device(): lax.all_to_all(slot_rows, 'ep', split_axis=0, concat_axis=0, tiled=True)  30.7 us
    all_to_all x1, waiting for transfers between devices, on_device(): lax.all_to_all(summed, 'ep', split_axis=0, concat_axis=0, tiled=True)  17.5 us
    dot_general x1, matrix products, on_device(): jnp.einsum('aecf,efd->aecd', hidden_units, down_weight, preferred_element...  16.6 us
    reshape x1, local copies, waits for them, and re-layouts, on_device(): partial_value.reshape(tp_size, ep_size * local_experts * capacity, -1)  16.3 us
    convert_element_type x1, local copies, waits for them, and re-layouts, on_device(): partial_value = jnp.einsum('aecf,efd->aecd', hidden_units, down_weight, p...  11.4 us
  transfers between devices with their start and end apart: 4, of which 3 were waited for; matrix products, arithmetic and copies ran while one was open for 2% of the time, Pallas kernels for 0%

profile of v1, /device:TPU:24, one launch (start us, length us, event | category | flops | bytes accessed | tf_op | source)
XLA Modules:
  0.0 482.6 jit_solution(5891827594901361238)
XLA Ops:
  7.2 0.8 copy.42
  8.6 0.4 fusion.36
  8.9 1.0 fusion.60
  10.0 1.2 fusion.6
  11.6 30.7 %all_to_all.20 = bf16[32,1,3,2048]{3,2,1,0:T(4,128)(2,1)S(1)} all-to-all(bf16[32,1,3,2048]{3,2,1,0:T(4,128)(2,1)S(1)} %copy.46), channel_id=1, replica_groups=mesh['ep'=32,'tp'=16] {'ep'}, dimensions={0} | all-to-all | bytes 786432 | tf_op jit(solution)/shard_map/all_to_all | solution.py:154
  46.8 190.8 %all_to_all.21 = bf16[512,1,3,2048]{3,2,1,0:T(4,128)(2,1)S(1)} all-to-all(bf16[512,1,3,2048]{3,2,1,0:T(4,128)(2,1)S(1)} %constant_dynamic-update-slice_fusion), channel_id=1, replica_groups=mesh['ep'=32,'tp'=16] {'tp'}, dimensions={0} | all-to-all | bytes 12582912 | tf_op jit(solution)/shard_map/all_to_all | solution.py:16
  237.5 3.2 copy-done.1
  240.8 6.9 %fusion.25 = f32[512,1,3,128]{3,0,2,1:T(8,128)S(1)} fusion(bf16[512,1,3,2048]{3,2,1,0:T(4,128)(2,1)S(1)} %all_to_all.21, bf16[1,2048,128]{2,1,0:T(8,128)(2,1)S(1)} %copy-done.8), kind=kOutput, calls=%fused_computation.21 | convolution fusion | flops 805502976 | bytes 7602176 | tf_op jit(solution)/shard_map/aecd,edf->aecf/dot_general | solution.py:105
  247.7 16.6 %convert_bitcast_fusion = bf16[512,1,3,2048]{3,0,2,1:T(8,128)(2,1)} fusion(bf16[512,1,3,2048]{3,2,1,0:T(4,128)(2,1)} %copy-done.1, f32[512,1,3,128]{3,0,2,1:T(8,128)S(1)} %fusion.25, bf16[1,128,2048]{2,1,0:T(8,128)(2,1)S(1)} %copy-done.9, bf16[1,2048,128]{2,1,0:T(8,128)(2,1)S(1)} %copy-done.10), kind=kOutput, calls=%fused_computation.4 | convolution fusion | flops 1615527936 | bytes 14417920 | tf_op jit(solution)/shard_map/aecf,efd->aecd/dot_general | solution.py:156
  264.3 11.4 %copy.48 = bf16[512,1,3,2048]{3,2,0,1:T(4,128)(2,1)} copy(bf16[512,1,3,2048]{3,0,2,1:T(8,128)(2,1)} %convert_bitcast_fusion) | data formatting | bytes 12582912 | tf_op jit(solution)/shard_map/convert_element_type | solution.py:158
  275.7 16.3 %reshape.224 = bf16[16,96,2048]{2,1,0:T(8,128)(2,1)} reshape(bf16[512,1,3,2048]{3,2,0,1:T(4,128)(2,1)} %copy.48) | data formatting | bytes 12582912 | tf_op jit(solution)/shard_map/reshape | solution.py:159
  292.1 5.6 %all-to-all-start.2 = ((bf16[16,96,2048]{2,1,0:T(8,128)(2,1)}), bf16[16,96,2048]{2,1,0:T(8,128)(2,1)}, u32[]{:S(2)}, u32[]{:S(2)}) async-start(bf16[16,96,2048]{2,1,0:T(8,128)(2,1)} %reshape.224), calls=%async_computation.3 | async-start | bytes 12582912 | tf_op jit(solution)/shard_map/all_to_all | solution.py:160
  298.2 2.8 collective-permute-start
  301.6 0.9 collective-permute-done
  302.6 0.5 fusion.107
  303.5 0.4 fusion.35
  304.0 2.1 convolution_convert_fusion
  306.1 140.8 %all-to-all-done.2 = bf16[16,96,2048]{2,1,0:T(8,128)(2,1)} async-done(((bf16[16,96,2048]{2,1,0:T(8,128)(2,1)}), bf16[16,96,2048]{2,1,0:T(8,128)(2,1)}, u32[]{:S(2)}, u32[]{:S(2)}) %all-to-all-start.2) | async-done | bytes 6291488 | tf_op jit(solution)/shard_map/all_to_all | solution.py:160
  446.9 4.1 reduce_sum.76
  451.0 1.0 reshape.225
  452.0 4.6 all-to-all-start.3
  456.8 0.4 fusion.86
  457.2 17.5 %all-to-all-done.3 = bf16[32,3,2048]{2,1,0:T(4,128)(2,1)S(1)} async-done(((bf16[32,3,2048]{2,1,0:T(4,128)(2,1)}), bf16[32,3,2048]{2,1,0:T(4,128)(2,1)S(1)}, u32[]{:S(2)}, u32[]{:S(2)}) %all-to-all-start.3) | async-done | bytes 393248 | tf_op jit(solution)/shard_map/all_to_all | solution.py:163
  474.7 1.1 fusion.7
  (79 shorter events, 7.1 us)
Async XLA Ops:
  7.2 296.8 %copy-start = (bf16[192,2048]{1,0:T(8,128)(2,1)S(1)}, bf16[192,2048]{1,0:T(8,128)(2,1)}, u32[]{:S(2)}) copy-start(bf16[192,2048]{1,0:T(8,128)(2,1)} %param.20) | copy-start | bytes 2359300
  46.8 194.0 %copy-start.8 = (bf16[1,2048,128]{2,1,0:T(8,128)(2,1)S(1)}, bf16[1,2048,128]{2,1,0:T(8,128)(2,1)}, u32[]{:S(2)}) copy-start(bf16[1,2048,128]{2,1,0:T(8,128)(2,1)} %param.25) | copy-start | bytes 1572868
  237.5 3.2 copy-start.1
  240.8 6.9 %copy-start.9 = (bf16[1,128,2048]{2,1,0:T(8,128)(2,1)S(1)}, bf16[1,128,2048]{2,1,0:T(8,128)(2,1)}, u32[]{:S(2)}) copy-start(bf16[1,128,2048]{2,1,0:T(8,128)(2,1)} %param.27) | copy-start | bytes 1572868
  240.8 6.9 %copy-start.10 = (bf16[1,2048,128]{2,1,0:T(8,128)(2,1)S(1)}, bf16[1,2048,128]{2,1,0:T(8,128)(2,1)}, u32[]{:S(2)}) copy-start(bf16[1,2048,128]{2,1,0:T(8,128)(2,1)} %param.26) | copy-start | bytes 1572868
  292.0 5.9 %copy-start.3 = (bf16[512,64]{0,1:T(8,128)(2,1)S(1)}, bf16[512,64]{0,1:T(8,128)(2,1)}, u32[]{:S(2)}) copy-start(bf16[512,64]{0,1:T(8,128)(2,1)} %param.15) | copy-start | bytes 196612
  292.0 6.0 %copy-start.6 = (f32[1,64]{1,0:T(1,128)S(1)}, f32[1,64]{1,0:T(1,128)}, u32[]{:S(2)}) copy-start(f32[1,64]{1,0:T(1,128)} %param.18) | copy-start | bytes 772
  292.0 6.1 %copy-start.4 = (bf16[512,64]{0,1:T(8,128)(2,1)S(1)}, bf16[512,64]{0,1:T(8,128)(2,1)}, u32[]{:S(2)}) copy-start(bf16[512,64]{0,1:T(8,128)(2,1)} %param.16) | copy-start | bytes 196612
  292.0 8.9 %copy-start.2 = (bf16[512,192]{0,1:T(8,128)(2,1)S(1)}, bf16[512,192]{0,1:T(8,128)(2,1)}, u32[]{:S(2)}) copy-start(bf16[512,192]{0,1:T(8,128)(2,1)} %param.14) | copy-start | bytes 589828
  292.0 10.5 %copy-start.11 = (f32[3,64]{1,0:T(4,128)S(1)}, f32[3,64]{1,0:T(4,128)}, u32[]{:S(2)}) copy-start(f32[3,64]{1,0:T(4,128)} %param.17) | copy-start | bytes 2308
  292.1 11.0 %copy-start.7 = (f32[3]{0:T(128)S(1)}, f32[3]{0:T(128)}, u32[]{:S(2)}) copy-start(f32[3]{0:T(128)} %param.19) | copy-start | bytes 40
  292.1 154.8 %all-to-all-start.2 = ((bf16[16,96,2048]{2,1,0:T(8,128)(2,1)}), bf16[16,96,2048]{2,1,0:T(8,128)(2,1)}, u32[]{:S(2)}, u32[]{:S(2)}) async-start(bf16[16,96,2048]{2,1,0:T(8,128)(2,1)} %reshape.224), calls=%async_computation.3 | async-start | bytes 12582912 | tf_op jit(solution)/shard_map/all_to_all | solution.py:160
  297.7 178.1 %reduce-scatter.2.cloned.1.call-start = ((), (), s32[]{:S(2)}) async-start(), calls=%async_computation.5 | async-start | bytes 2228224 | tf_op jit(solution)/shard_map/reduce_scatter | solution.py:129
  298.2 4.4 collective-permute-start
  303.4 153.3 %copy-start.5 = (f32[32,2]{0,1:T(2,128)S(1)}, f32[32,2]{0,1:T(2,128)}, u32[]{:S(2)}) copy-start(f32[32,2]{0,1:T(2,128)} %param.24) | copy-start | bytes 772
  452.0 22.7 %all-to-all-start.3 = ((bf16[32,3,2048]{2,1,0:T(4,128)(2,1)}), bf16[32,3,2048]{2,1,0:T(4,128)(2,1)S(1)}, u32[]{:S(2)}, u32[]{:S(2)}) async-start(bf16[32,3,2048]{2,1,0:T(4,128)(2,1)} %reshape.225), calls=%async_computation.4 | async-start | bytes 1048576 | tf_op jit(solution)/shard_map/all_to_all | solution.py:163
Sparse Core Ops, SparseCore 0:
  306.3 131.9 reduce-scatter.1
